TPU v7x, 1024 devices: a whole 8x8x8 slice. The times are simulated.
1024 devices in a mesh: row: 64 (over z, y), col: 16 (over x, core).
Axes of the slice: x: 8, y: 8, z: 8, core: 2. Of those that a mesh axis runs over, the one named last changes fastest.
Arguments:
- tokens: bfloat16 [32768, 2048], P('row'), may hold values from -6 to 6
- outer_weight: bfloat16 [2048, 1024], P(None, 'col'), may hold values from -0.125 to 0.125
- inner_weight: bfloat16 [2048, 1024], P(None, 'col'), may hold values from -0.125 to 0.125
- value_weight: bfloat16 [2048, 1024], P(None, 'col'), may hold values from -0.125 to 0.125
- conv_taps: float32 [3, 3, 1024], P(None, None, 'col'), may hold values from -3.5 to 3.5
- feature_weight: float32 [33, 128], replicated, may hold values from -1 to 1
- feature_phase: float32 [128], replicated, may hold values from -3.140625 to 3.140625
- inner_mats: float32 [2, 128, 128], replicated, may hold values from -0.5 to 0.5
- inner_phase: float32 [2, 128], replicated, may hold values from -3.140625 to 3.140625
- frequency: float32 [128], replicated, may hold values from 0.1 to 1.9
- forward_weight: float32 [128, 1024], P(None, 'col'), may hold values from -0.5 to 0.5
- backward_weight: float32 [128, 1024], P(None, 'col'), may hold values from -0.5 to 0.5
- decay_rate: float32 [1024], P('col'), may hold values from 0.2 to 3276.8, as said below
- skip_gain: float32 [1024], P('col'), may hold values from -6 to 6
- output_weight: bfloat16 [1024, 2048], replicated, may hold values from -0.1875 to 0.1875
Outputs:
- layer_out: bfloat16 [32768, 2048], P(('row', 'col'))
Inputs may be any that keep to these rules, and one draw needn't show every extreme that they name: `decay_rate`: positive rates of the channels' filter windows.
All inputs are finite; a program needn't handle non-finite values.
Results may differ from a plain program's by a relative error of at most 0.014.
Values may be sent and summed in bfloat16 or wider, within the bound.
A program may use at most 64 MiB of HBM per device.

v0:
```python
import functools
import math

import jax
import jax.numpy as jnp
import numpy as np
from jax import lax
from jax.experimental import pallas as pl
from jax.experimental.pallas import tpu as pltpu
from jax.sharding import PartitionSpec as P

BANDS = 16
INNER = 2
LANES = 128
MESH = pl.DeviceIdType.MESH
PRECISE = lax.Precision.HIGHEST
F32 = jnp.float32
BF16 = jnp.bfloat16


def tables(row_blocks):
    total = 2 * row_blocks * LANES
    k = np.arange(row_blocks)
    r = np.arange(row_blocks)
    b = np.arange(LANES)
    outer = (np.outer(2 * k + 1, r) % (4 * row_blocks)) * (2.0 * math.pi / (4 * row_blocks))
    one = np.concatenate([np.cos(outer), np.sin(outer)], axis=0)
    one_back = np.concatenate([np.cos(outer).T, -np.sin(outer).T], axis=1)
    inner = (np.outer(b, b) % LANES) * (2.0 * math.pi / LANES)
    c, s = np.cos(inner), np.sin(inner)
    two = np.block([[c, -s], [s, c]])
    two_back = np.block([[c, s], [-s, c]])
    twist = np.outer(2 * k + 1, b) * (math.pi / total)
    return (
        jnp.asarray(one, BF16),
        jnp.asarray(one_back, BF16),
        jnp.asarray(two, BF16),
        jnp.asarray(two_back, BF16),
        jnp.asarray(np.stack([np.cos(twist), np.sin(twist)]), F32),
    )


def mm(a, b):
    return jnp.dot(a, b, preferred_element_type=F32)


def kernel(rows, cols, seq_length, *refs):
    (
        tokens, outer_w, inner_w, value_w, taps_h, first_h, phase_h, mats_h, iphase_h, freq_h,
        ahead_h, behind_h, rate_h, skip_h, map_h, one_h, one_back_h, two_h, two_back_h, twist_h,
        out_ref,
        tok, w_o, w_i, w_v, taps, first, phase, mats, iphase, freq, ahead_w, behind_w, rate, skip,
        out_w, one, one_back, two, two_back, twist,
        proj, gate_s, sig_s, f_send, f_recv, s_send, s_recv, y_send, y_recv, m_send, m_recv,
        load_sem, halo_send, halo_recv, a2a_send, a2a_recv,
    ) = refs
    me_r, me_c = lax.axis_index("row"), lax.axis_index("col")
    length = tok.shape[0]
    width = w_o.shape[1]
    subs = length // LANES
    chunks = 4
    step = length // chunks

    def load(src, dst, index):
        copy = pltpu.make_async_copy(src, dst, load_sem.at[index])
        copy.start()
        return copy

    small = [
        load(s, d, i)
        for i, (s, d) in enumerate(
            [
                (first_h, first), (phase_h, phase), (mats_h, mats), (iphase_h, iphase), (freq_h, freq),
                (ahead_h, ahead_w), (behind_h, behind_w), (rate_h, rate),
            ]
        )
    ]
    weights = [load(s, d, 8 + i) for i, (s, d) in enumerate([(inner_w, w_i), (outer_w, w_o), (value_w, w_v)])]
    token_loads = [
        load(tokens.at[pl.ds(c * step, step)], tok.at[pl.ds(c * step, step)], 11 + c) for c in range(chunks)
    ]

    barrier = pltpu.get_barrier_semaphore()

    def greet_row(d, carry):
        peer = lax.rem(me_r + d, rows)
        pl.semaphore_signal(barrier, inc=1, device_id=(peer, me_c), device_id_type=MESH)
        return carry

    def greet_col(d, carry):
        peer = lax.rem(me_c + d, cols)
        pl.semaphore_signal(barrier, inc=1, device_id=(me_r, peer), device_id_type=MESH)
        return carry

    lax.fori_loop(1, rows, greet_row, 0)
    lax.fori_loop(1, cols, greet_col, 0)

    for copy in small:
        copy.wait()
    place = me_r * length + lax.broadcasted_iota(jnp.int32, (length, LANES), 0)
    lane = lax.broadcasted_iota(jnp.int32, (length, LANES), 1)
    is_sine = lane > BANDS
    band = 1 + jnp.where(is_sine, lane - (BANDS + 1), lane - 1) * (seq_length // (4 * BANDS))
    turns = (place * band + jnp.where(is_sine, seq_length // 4, 0)) & (seq_length - 1)
    waves = jnp.cos(2.0 * math.pi / seq_length * turns.astype(F32))
    scaled = place.astype(F32) / (seq_length - 1)
    features = jnp.where(lane == 0, scaled, waves)[:, : 2 * BANDS + 1]
    hidden = jnp.sin(freq[...] * (jnp.dot(features, first[...], precision=PRECISE, preferred_element_type=F32) + phase[...]))
    for level in range(INNER):
        hidden = jnp.sin(
            freq[...]
            * (jnp.dot(hidden, mats[level], precision=PRECISE, preferred_element_type=F32) + iphase[level : level + 1, :])
        )
    both = jnp.concatenate([ahead_w[...], behind_w[...]], axis=1)
    rates = jnp.concatenate([rate[...], rate[...]], axis=1)
    filters = jnp.dot(hidden, both, precision=PRECISE, preferred_element_type=F32) * jnp.exp(
        -scaled[:, : 2 * width] * rates
    )
    filters = jnp.where((place[:, : 2 * width] == 0) & (lane[:, : 2 * width] >= width), 0.0, filters)
    turned = filters.T
    fa, fb = turned[:width], turned[width:]
    f_send[...] = jnp.concatenate([fa + fb, fa - fb], axis=1).reshape(width, 2 * subs, LANES).astype(BF16)

    for copy in weights:
        copy.wait()
    joined = jnp.concatenate([w_i[...], w_o[...], w_v[...]], axis=1)
    for c in range(chunks):
        token_loads[c].wait()
        part = mm(tok[pl.ds(c * step, step), :], joined)
        proj[pl.ds(8 + c * step, step), :] = part.astype(BF16).astype(F32)

    late = [
        load(s, d, 11 + chunks + i)
        for i, (s, d) in enumerate(
            [
                (taps_h, taps), (skip_h, skip), (one_h, one), (two_h, two), (twist_h, twist),
                (two_back_h, two_back), (one_back_h, one_back), (map_h, out_w),
            ]
        )
    ]

    pl.semaphore_wait(barrier, rows + cols - 2)

    after, before = lax.rem(me_r + 1, rows), lax.rem(me_r + rows - 1, rows)
    up = pltpu.make_async_remote_copy(
        proj.at[pl.ds(length, 8)], proj.at[pl.ds(0, 8)], halo_send.at[0], halo_recv.at[0],
        device_id=(after, me_c), device_id_type=MESH,
    )
    down = pltpu.make_async_remote_copy(
        proj.at[pl.ds(8, 8)], proj.at[pl.ds(8 + length, 8)], halo_send.at[1], halo_recv.at[1],
        device_id=(before, me_c), device_id_type=MESH,
    )
    up.start()
    down.start()

    def scatter(send, recv, index):
        def one_peer(d, carry):
            peer = lax.rem(me_r + d, rows)
            pltpu.make_async_remote_copy(
                send.at[peer], recv.at[me_r], a2a_send.at[index], a2a_recv.at[index],
                device_id=(peer, me_c), device_id_type=MESH,
            ).start()
            return carry

        lax.fori_loop(1, rows, one_peer, 0)
        recv[me_r] = send[me_r]

    def drain(ref, count, sem):
        pltpu.make_async_copy(ref.at[pl.ds(0, count)], ref.at[pl.ds(0, count)], sem).wait()

    scatter(f_send, f_recv, 0)

    for copy in late[:2]:
        copy.wait()
    up.wait()
    down.wait()
    proj[7:8, :] = jnp.where(me_r == 0, 0.0, proj[7:8, :])
    proj[8 + length : 9 + length, :] = jnp.where(me_r == rows - 1, 0.0, proj[8 + length : 9 + length, :])
    tap = [
        jnp.concatenate([taps[a, 1:2, :], taps[a, 0:1, :], taps[a, 2:3, :]], axis=1) for a in range(3)
    ]
    conv = proj[7 : 7 + length, :] * tap[0] + proj[8 : 8 + length, :] * tap[1] + proj[9 : 9 + length, :] * tap[2]
    signal = (conv[:, :width] * conv[:, 2 * width :]).astype(BF16).astype(F32)
    gate_s[...] = conv[:, width : 2 * width].astype(BF16).astype(F32)
    sig_s[...] = signal
    s_send[...] = signal.T.reshape(width, subs, LANES).astype(BF16)
    scatter(s_send, s_recv, 1)

    half = rows * subs
    for copy in late[2:5]:
        copy.wait()
    twist_c, twist_s = twist[0], twist[1]

    def first_stage(x):
        turned = mm(one[...], x)
        real, imag = turned[:half], turned[half:]
        return jnp.concatenate(
            [real * twist_c - imag * twist_s, -(imag * twist_c + real * twist_s)], axis=1
        ).astype(BF16)

    drain(f_recv, rows - 1, a2a_recv.at[0])
    got = f_recv[...].astype(F32)
    plus = got[:, :subs].reshape(half, LANES)
    minus = got[:, subs:].reshape(half, LANES)
    energy = jnp.sum(plus * plus + minus * minus, axis=0, keepdims=True)
    scale = lax.rsqrt(1.0 + 0.5 * jnp.sum(energy, axis=1, keepdims=True)) * (1.0 / (half * LANES))
    spec_real = mm(first_stage(plus.astype(BF16)), two[:, :LANES]) * scale
    spec_imag = mm(first_stage(minus.astype(BF16)), two[:, LANES:]) * scale

    for copy in late[5:7]:
        copy.wait()
    drain(s_recv, rows - 1, a2a_recv.at[1])
    spec = mm(first_stage(s_recv[...].astype(F32).reshape(half, LANES).astype(BF16)), two[...])
    real, imag = spec[:, :LANES], spec[:, LANES:]
    product = jnp.concatenate(
        [real * spec_real - imag * spec_imag, real * spec_imag + imag * spec_real], axis=1
    ).astype(BF16)
    back = mm(product, two_back[...])
    real, imag = back[:, :LANES], back[:, LANES:]
    untwisted = jnp.concatenate(
        [real * twist_c - imag * twist_s, imag * twist_c + real * twist_s], axis=0
    ).astype(BF16)
    response = mm(one_back[...], untwisted)
    y_send[...] = response.reshape(rows, subs, LANES).astype(BF16)
    scatter(y_send, y_recv, 2)

    skipped = skip[...] * sig_s[...]
    drain(y_recv, rows - 1, a2a_recv.at[2])
    replied = y_recv[...].astype(F32).reshape(width, length).T
    mixed = (gate_s[...] * (replied + skipped)).astype(BF16)
    m_send[...] = mixed.reshape(cols, length // cols, width)

    def col_peer(d, carry):
        peer = lax.rem(me_c + d, cols)
        pltpu.make_async_remote_copy(
            m_send.at[peer], m_recv.at[me_c], a2a_send.at[3], a2a_recv.at[3],
            device_id=(me_r, peer), device_id_type=MESH,
        ).start()
        return carry

    lax.fori_loop(1, cols, col_peer, 0)
    m_recv[me_c] = m_send[me_c]
    late[7].wait()
    drain(m_recv, cols - 1, a2a_recv.at[3])
    whole = jnp.concatenate([m_recv[j] for j in range(cols)], axis=1)
    tile = min(512, out_ref.shape[1])
    for c in range(out_ref.shape[1] // tile):
        out_ref[:, c * tile : (c + 1) * tile] = mm(whole, out_w[:, c * tile : (c + 1) * tile]).astype(BF16)

    drain(f_send, rows - 1, a2a_send.at[0])
    drain(s_send, rows - 1, a2a_send.at[1])
    drain(y_send, rows - 1, a2a_send.at[2])
    drain(m_send, cols - 1, a2a_send.at[3])


def on_device(rows, cols, *args):
    (
        tokens, outer_weight, inner_weight, value_weight, conv_taps, feature_weight, feature_phase, inner_mats,
        inner_phase, frequency, forward_weight, backward_weight, decay_rate, skip_gain, output_weight,
    ) = args
    length, model = tokens.shape
    width = outer_weight.shape[1]
    units = frequency.shape[0]
    subs = length // LANES
    seq_length = length * rows
    out_rows = length // cols
    operands = (
        tokens, outer_weight, inner_weight, value_weight, conv_taps, feature_weight, feature_phase.reshape(1, units),
        inner_mats, inner_phase, frequency.reshape(1, units), forward_weight, backward_weight,
        decay_rate.reshape(1, width), skip_gain.reshape(1, width), output_weight,
    ) + tables(rows * subs)
    slab = lambda n: pltpu.VMEM((rows, n, LANES), BF16)
    scratch = [pltpu.VMEM(x.shape, x.dtype) for x in operands] + [
        pltpu.VMEM((length + 16, 3 * width), F32),
        pltpu.VMEM((length, width), F32),
        pltpu.VMEM((length, width), F32),
        slab(2 * subs), slab(2 * subs), slab(subs), slab(subs), slab(subs), slab(subs),
        pltpu.VMEM((cols, out_rows, width), BF16),
        pltpu.VMEM((cols, out_rows, width), BF16),
        pltpu.SemaphoreType.DMA((24,)),
        pltpu.SemaphoreType.DMA((2,)),
        pltpu.SemaphoreType.DMA((2,)),
        pltpu.SemaphoreType.DMA((4,)),
        pltpu.SemaphoreType.DMA((4,)),
    ]
    return pl.pallas_call(
        functools.partial(kernel, rows, cols, seq_length),
        out_shape=jax.ShapeDtypeStruct((out_rows, model), BF16),
        in_specs=[pl.BlockSpec(memory_space=pl.ANY)] * len(operands),
        out_specs=pl.BlockSpec(memory_space=pltpu.VMEM),
        scratch_shapes=scratch,
        compiler_params=pltpu.CompilerParams(
            collective_id=0, has_side_effects=True, vmem_limit_bytes=56 * 1024 * 1024
        ),
    )(*operands)


def solution(mesh):
    placed = (
        P("row", None),
        P(None, "col"),
        P(None, "col"),
        P(None, "col"),
        P(None, None, "col"),
        P(),
        P(),
        P(),
        P(),
        P(),
        P(None, "col"),
        P(None, "col"),
        P("col"),
        P("col"),
        P(),
    )
    return jax.shard_map(
        functools.partial(on_device, mesh.shape["row"], mesh.shape["col"]),
        mesh=mesh, in_specs=placed, out_specs=P(("row", "col"), None), check_vma=False,
    )
```

profile of v0, /device:TPU:1, one launch (start us, length us, event | category | flops | bytes accessed | tf_op | source)
XLA Modules:
  0.0 67.4 jit_solution(11006358206668182538)
XLA Ops:
  0.0 1.5 %copy.24.refs_10_ = f32[128,64]{1,0:T(8,128)} copy(f32[128,64]{0,1:T(8,128)} %param.30) | data formatting | bytes 65536 | tf_op args[10]
  1.5 1.5 %copy.25.refs_11_ = f32[128,64]{1,0:T(8,128)} copy(f32[128,64]{0,1:T(8,128)} %param.31) | data formatting | bytes 65536 | tf_op args[11]
  3.0 1.9 %copy.21.refs_1_ = bf16[2048,64]{1,0:T(8,128)(2,1)} copy(bf16[2048,64]{0,1:T(8,128)(2,1)} %param.21) | data formatting | bytes 524288 | tf_op args[1]
  4.9 2.0 %copy.22.refs_2_ = bf16[2048,64]{1,0:T(8,128)(2,1)} copy(bf16[2048,64]{0,1:T(8,128)(2,1)} %param.22) | data formatting | bytes 524288 | tf_op args[2]
  6.9 2.0 %copy.23.refs_3_ = bf16[2048,64]{1,0:T(8,128)(2,1)} copy(bf16[2048,64]{0,1:T(8,128)(2,1)} %param.23) | data formatting | bytes 524288 | tf_op args[3]
  8.9 57.0 %shard_map.190 = bf16[32,2048]{1,0:T(8,128)(2,1)} custom-call(bf16[512,2048]{1,0:T(8,128)(2,1)} %refs_0_.1, bf16[2048,64]{1,0:T(8,128)(2,1)} %copy.21.refs_1_, bf16[2048,64]{1,0:T(8,128)(2,1)} %copy.22.refs_2_, bf16[2048,64]{1,0:T(8,128)(2,1)} %copy.23.refs_3_, f32[3,3,64]{2,1,0:T(4,128)} %refs_4_.1, f32[33,128]{1,0:T(8,128)} %refs_5_.1, f32[1,128]{1,0:T(1,128)} %bitcast.4, ...), custom_call_target="tpu_custom_call" | custom-call | tf_op jit(solution)/shard_map/pallas_call | solution.py:286
  65.8 1.6 %copy.27 = bf16[32,2048]{1,0:T(8,128)(2,1)} copy(bf16[32,2048]{1,0:T(8,128)(2,1)} %shard_map.190) | data formatting | bytes 262144
where the time goes:
time: 67.8 us; the launch traced here: 67.4 us
  Pallas kernels  57 us (84%)
  local copies, waits for them, and re-layouts  10.4 us (15%)
    pallas_call x1, Pallas kernels, on_device(): pl.pallas_call(functools.partial(kernel, rows, cols, seq_length), out_sha...  57 us
    unnamed x6, local copies, waits for them, and re-layouts  10.4 us

commit v1 on v0

v1 whole, which is shorter than its diff:
```python
import functools
import math

import jax
import jax.numpy as jnp
import numpy as np
from jax import lax
from jax.experimental import pallas as pl
from jax.experimental.pallas import tpu as pltpu
from jax.sharding import PartitionSpec as P

BANDS = 16
INNER = 2
LANES = 128
MESH = pl.DeviceIdType.MESH
F32 = jnp.float32
BF16 = jnp.bfloat16


def tables(row_blocks):
    total = 2 * row_blocks * LANES
    k = np.arange(row_blocks)
    r = np.arange(row_blocks)
    b = np.arange(LANES)
    outer = (np.outer(2 * k + 1, r) % (4 * row_blocks)) * (2.0 * math.pi / (4 * row_blocks))
    one = np.concatenate([np.cos(outer), np.sin(outer)], axis=0)
    one_back = np.concatenate([np.cos(outer).T, -np.sin(outer).T], axis=1)
    inner = (np.outer(b, b) % LANES) * (2.0 * math.pi / LANES)
    c, s = np.cos(inner), np.sin(inner)
    two = np.block([[c, -s], [s, c]])
    two_back = np.block([[c, s], [-s, c]])
    twist = np.outer(2 * k + 1, b) * (math.pi / total)
    return (
        jnp.asarray(one, BF16),
        jnp.asarray(one_back, BF16),
        jnp.asarray(two, BF16),
        jnp.asarray(two_back, BF16),
        jnp.asarray(np.stack([np.cos(twist), np.sin(twist)]), F32),
    )


def mm(a, b):
    return jnp.dot(a, b, preferred_element_type=F32)


def mm_t(a, b):
    return lax.dot_general(a, b, (((1,), (1,)), ((), ())), preferred_element_type=F32)


def split(x):
    high = x.astype(BF16)
    return high, (x - high.astype(F32)).astype(BF16)


def sine_near(x):
    x = jnp.maximum(jnp.minimum(x, math.pi - x), -math.pi - x)
    y = x * x
    p = y * (2.6083159809786593e-6) - 1.9810690719168633e-4
    p = p * y + 8.333078585565090e-3
    p = p * y - 1.6666659712791443e-1
    return x + x * (y * p)


def sine(x):
    turns = jnp.round(x * (0.5 / math.pi))
    x = x - turns * 6.28125
    x = x - turns * 1.93500518798828125e-3
    x = x - turns * 3.0199159819567530e-7
    return sine_near(x)


def spread(i, size):
    return size // 2 + ((i + 1) // 2) * (1 - 2 * lax.rem(i, 2))


def kernel(rows, cols, seq_length, *refs):
    (
        tokens, outer_w, inner_w, value_w, taps_h, first_h, phase_h, mats_h, iphase_h, freq_h,
        ahead_h, behind_h, rate_h, skip_h, map_h, one_h, one_back_h, two_h, two_back_h, twist_h,
        out_ref,
        tok, w_all, taps, first, phase, mats, iphase, freq, both, rate, skip,
        out_w, one, one_back, two, two_back, twist,
        proj, gate_s, sig_s, f_send, f_recv, s_send, s_recv, y_send, y_recv, m_send, m_recv,
        load_sem, halo_send, halo_recv, a2a_send, a2a_recv,
    ) = refs
    me_r, me_c = lax.axis_index("row"), lax.axis_index("col")
    length = tok.shape[0]
    width = w_all.shape[0] // 3
    subs = length // LANES
    zone = rows // 2
    per = width // zone
    ring = 8 if rows % 8 == 0 else 2
    me_z, me_y = me_r // ring, lax.rem(me_r, ring)
    after, before = lax.rem(me_r + 1, rows), lax.rem(me_r + rows - 1, rows)
    in_zone = me_r < zone

    def load(src, dst, index):
        copy = pltpu.make_async_copy(src, dst, load_sem.at[index])
        copy.start()
        return copy

    small = [
        load(s, d, i)
        for i, (s, d) in enumerate(
            [
                (first_h, first), (phase_h, phase), (mats_h, mats), (iphase_h, iphase), (freq_h, freq),
                (ahead_h, both.at[pl.ds(0, width)]), (behind_h, both.at[pl.ds(width, width)]), (rate_h, rate),
            ]
        )
    ]
    weights = [load(w, w_all.at[pl.ds(i * width, width)], 8 + i) for i, w in enumerate((inner_w, value_w, outer_w))]
    token_load = load(tokens, tok, 11)

    barrier = pltpu.get_barrier_semaphore()

    def greet(row, col):
        pl.semaphore_signal(barrier, inc=1, device_id=(row, col), device_id_type=MESH)

    @pl.when(in_zone)
    def _():
        def greet_row(d, carry):
            greet(lax.rem(me_r + d, rows), me_c)
            return carry

        lax.fori_loop(1, rows, greet_row, 0)

    @pl.when(me_r >= zone)
    def _():
        greet(before, me_c)
        greet(after, me_c)

    def greet_col(i, carry):
        greet(me_r, lax.rem(me_c + spread(i, cols), cols))
        return carry

    lax.fori_loop(0, cols - 1, greet_col, 0)

    for copy in small:
        copy.wait()

    @pl.when(in_zone)
    def _():
        lane = lax.broadcasted_iota(jnp.int32, (length, LANES), 1)
        is_sine = lane > BANDS
        band = 1 + jnp.where(is_sine, lane - (BANDS + 1), lane - 1) * (seq_length // (4 * BANDS))
        shift = jnp.where(is_sine, seq_length, seq_length * 3 // 4)
        rates = jnp.broadcast_to(jnp.concatenate([rate[...], rate[...]], axis=1), (2 * width, 2 * width)).T[:, :1]
        behind = lax.broadcasted_iota(jnp.int32, (2 * width, length), 0) >= width
        w_first, w_mats, w_both = split(first[...]), split(mats[...]), split(both[...])

        def dot3(x, w, multiply):
            x_high, x_low = split(x)
            return multiply(x_high, w[0]) + (multiply(x_low, w[0]) + multiply(x_high, w[1]))

        for block in range(2):
            start = (me_r + block * zone) * length
            place = start + lax.broadcasted_iota(jnp.int32, (length, LANES), 0)
            turns = ((place * band + shift) & (seq_length - 1)) - seq_length // 2
            waves = sine_near(turns.astype(F32) * (2.0 * math.pi / seq_length))
            features = jnp.where(lane == 0, place.astype(F32) / (seq_length - 1), waves)[:, : 2 * BANDS + 1]
            hidden = sine(freq[...] * (dot3(features, w_first, mm) + phase[...]))
            for level in range(INNER):
                mat = (w_mats[0][level], w_mats[1][level])
                hidden = sine(freq[...] * (dot3(hidden, mat, mm) + iphase[level : level + 1, :]))
            turned = dot3(hidden, w_both, lambda h, w: mm_t(w, h))
            lag = start + lax.broadcasted_iota(jnp.int32, (2 * width, length), 1)
            turned = turned * jnp.exp(-(lag.astype(F32) / (seq_length - 1)) * rates)
            turned = jnp.where((lag == 0) & behind, 0.0, turned)
            fa, fb = turned[:width], turned[width:]
            f_send[block] = (
                jnp.concatenate([fa + fb, fa - fb], axis=1).reshape(width, 2 * subs, LANES).astype(BF16)
            )

    for copy in weights:
        copy.wait()
    token_load.wait()
    part = mm_t(tok[...], w_all[...]).astype(BF16)
    proj[pl.ds(8, length), :] = part.astype(F32)
    turned = part[:, : 2 * width].astype(F32).T
    s_send[...] = (
        jnp.concatenate([turned[:width], turned[width:]], axis=1).reshape(width, 2 * subs, LANES).astype(BF16)
    )

    outside = me_r // zone
    pl.semaphore_wait(barrier, zone - 1 + outside + before // zone + after // zone + cols - 1)

    def push(src, dst, index, row):
        pltpu.make_async_remote_copy(
            src, dst, a2a_send.at[index], a2a_recv.at[index], device_id=(row, me_c), device_id_type=MESH
        ).start()

    def drain(ref, count, sem):
        pltpu.make_async_copy(ref.at[pl.ds(0, count)], ref.at[pl.ds(0, count)], sem).wait()

    mine = pl.ds(per * me_r, per)
    zone_z = zone // ring

    def signal_peer(i, carry):
        peer = lax.rem(me_z + i, zone_z) * ring + lax.rem(me_y + spread(i // zone_z, ring), ring)

        @pl.when(peer != me_r)
        def _():
            push(s_send.at[pl.ds(per * peer, per)], s_recv.at[me_r], 1, peer)

        return carry

    lax.fori_loop(0, zone, signal_peer, 0)

    @pl.when(in_zone)
    def _():
        s_recv[me_r] = s_send[mine]

        def filter_peer(d, carry):
            peer = lax.rem(me_r + d, zone)
            push(f_send.at[0, pl.ds(per * peer, per)], f_recv.at[me_r], 0, peer)
            push(f_send.at[1, pl.ds(per * peer, per)], f_recv.at[me_r + zone], 0, peer)
            return carry

        lax.fori_loop(1, zone, filter_peer, 0)
        f_recv[me_r] = f_send[0, mine]
        f_recv[me_r + zone] = f_send[1, mine]

    late = [
        load(s, d, 12 + i)
        for i, (s, d) in enumerate(
            [
                (taps_h, taps), (skip_h, skip), (one_h, one), (two_h, two), (twist_h, twist),
                (two_back_h, two_back), (one_back_h, one_back), (map_h, out_w),
            ]
        )
    ]

    up = pltpu.make_async_remote_copy(
        proj.at[pl.ds(length, 8)], proj.at[pl.ds(0, 8)], halo_send.at[0], halo_recv.at[0],
        device_id=(after, me_c), device_id_type=MESH,
    )
    down = pltpu.make_async_remote_copy(
        proj.at[pl.ds(8, 8)], proj.at[pl.ds(8 + length, 8)], halo_send.at[1], halo_recv.at[1],
        device_id=(before, me_c), device_id_type=MESH,
    )
    up.start()
    down.start()
    for copy in late[:7]:
        copy.wait()

    half = rows * subs
    @pl.when(in_zone)
    def _():
        twist_c, twist_s = twist[0], twist[1]

        def first_stage(parts):
            turned = mm(one[...], jnp.concatenate(parts, axis=1).astype(BF16))
            out = []
            for c in range(len(parts)):
                real = turned[:half, c * LANES : (c + 1) * LANES]
                imag = turned[half:, c * LANES : (c + 1) * LANES]
                out.append(
                    jnp.concatenate(
                        [real * twist_c - imag * twist_s, -(imag * twist_c + real * twist_s)], axis=1
                    ).astype(BF16)
                )
            return jnp.concatenate(out, axis=0)

        drain(f_recv, rows - 2, a2a_recv.at[0])
        got = [f_recv[:, c].astype(F32) for c in range(per)]
        plus = [x[:, :subs].reshape(half, LANES) for x in got]
        minus = [x[:, subs:].reshape(half, LANES) for x in got]
        spec_real = mm(first_stage(plus), two[:, :LANES])
        spec_imag = mm(first_stage(minus), two[:, LANES:])
        filters = []
        for c in range(per):
            energy = jnp.sum(plus[c] * plus[c] + minus[c] * minus[c], axis=0, keepdims=True)
            scale = lax.rsqrt(1.0 + 0.5 * jnp.sum(energy, axis=1, keepdims=True)) * (1.0 / (half * LANES))
            own = slice(c * half, (c + 1) * half)
            filters.append((spec_real[own] * scale, spec_imag[own] * scale))

        lane = lax.broadcasted_iota(jnp.int32, (half, LANES), 1)
        row = lax.broadcasted_iota(jnp.int32, (half, LANES), 0)
        channel = lax.broadcasted_iota(jnp.int32, (1, width), 1)

        def short_conv(x, which, c):
            left = pltpu.roll(x, 1, 1)
            left = jnp.where(lane == 0, pltpu.roll(left, 1, 0), left)
            left = jnp.where((lane == 0) & (row == 0), 0.0, left)
            right = pltpu.roll(x, LANES - 1, 1)
            right = jnp.where(lane == LANES - 1, pltpu.roll(right, half - 1, 0), right)
            right = jnp.where((lane == LANES - 1) & (row == half - 1), 0.0, right)
            tap = [
                jnp.sum(jnp.where(channel == per * me_r + c, taps[a, which : which + 1, :], 0.0), axis=1, keepdims=True)
                for a in range(3)
            ]
            return left * tap[0] + x * tap[1] + right * tap[2]

        drain(s_recv, rows - 1, a2a_recv.at[1])
        signals = []
        for c in range(per):
            raw = s_recv[:, c].astype(F32)
            signals.append(
                short_conv(raw[:, :subs].reshape(half, LANES), 1, c) * short_conv(raw[:, subs:].reshape(half, LANES), 2, c)
            )
        spec = mm(first_stage(signals), two[...])
        products = []
        for c in range(per):
            real, imag = spec[c * half : (c + 1) * half, :LANES], spec[c * half : (c + 1) * half, LANES:]
            f_real, f_imag = filters[c]
            products.append(
                jnp.concatenate([real * f_real - imag * f_imag, real * f_imag + imag * f_real], axis=1).astype(BF16)
            )
        back = mm(jnp.concatenate(products, axis=0), two_back[...])
        untwisted = []
        for c in range(per):
            real, imag = back[c * half : (c + 1) * half, :LANES], back[c * half : (c + 1) * half, LANES:]
            untwisted.append(
                jnp.concatenate(
                    [real * twist_c - imag * twist_s, imag * twist_c + real * twist_s], axis=0
                ).astype(BF16)
            )
        response = mm(one_back[...], jnp.concatenate(untwisted, axis=1))
        for c in range(per):
            y_send[:, c] = response[:, c * LANES : (c + 1) * LANES].reshape(rows, subs, LANES).astype(BF16)

        ring_z = rows // ring

        def response_peer(i, carry):
            peer = lax.rem(me_z + spread(lax.rem(i, ring_z), ring_z), ring_z) * ring + lax.rem(
                me_y + spread(i // ring_z, ring), ring
            )
            push(y_send.at[peer], y_recv.at[mine], 2, peer)
            return carry

        lax.fori_loop(0, rows - 1, response_peer, 0)
        y_recv[mine] = y_send[me_r]

    up.wait()
    down.wait()
    proj[7:8, :] = jnp.where(me_r == 0, 0.0, proj[7:8, :])
    proj[8 + length : 9 + length, :] = jnp.where(me_r == rows - 1, 0.0, proj[8 + length : 9 + length, :])
    tap = [
        jnp.concatenate([taps[a, 1:2, :], taps[a, 2:3, :], taps[a, 0:1, :]], axis=1) for a in range(3)
    ]
    conv = proj[7 : 7 + length, :] * tap[0] + proj[8 : 8 + length, :] * tap[1] + proj[9 : 9 + length, :] * tap[2]
    signal = (conv[:, :width] * conv[:, width : 2 * width]).astype(BF16).astype(F32)
    gate_s[...] = conv[:, 2 * width :].astype(BF16).astype(F32)
    sig_s[...] = skip[...] * signal
    late[7].wait()

    @pl.when(in_zone)
    def _():
        drain(y_recv, width - per, a2a_recv.at[2])

    @pl.when(me_r >= zone)
    def _():
        drain(y_recv, width, a2a_recv.at[2])

    replied = y_recv[...].astype(F32).reshape(width, length).T
    mixed = (gate_s[...] * (replied + sig_s[...])).astype(BF16)
    m_send[...] = mixed.reshape(cols, length // cols, width)

    def col_peer(i, carry):
        peer = lax.rem(me_c + spread(i, cols), cols)
        pltpu.make_async_remote_copy(
            m_send.at[peer], m_recv.at[me_c], a2a_send.at[3], a2a_recv.at[3],
            device_id=(me_r, peer), device_id_type=MESH,
        ).start()
        return carry

    lax.fori_loop(0, cols - 1, col_peer, 0)
    m_recv[me_c] = m_send[me_c]

    @pl.when(in_zone)
    def _():
        drain(s_send, width - per, a2a_send.at[1])
        drain(f_recv, rows - 2, a2a_send.at[0])
        drain(y_send, rows - 1, a2a_send.at[2])

    @pl.when(me_r >= zone)
    def _():
        drain(s_send, width, a2a_send.at[1])

    drain(m_recv, cols - 1, a2a_recv.at[3])
    whole = jnp.concatenate([m_recv[j] for j in range(cols)], axis=1)
    tile = min(512, out_ref.shape[1])
    for c in range(out_ref.shape[1] // tile):
        out_ref[:, c * tile : (c + 1) * tile] = mm(whole, out_w[:, c * tile : (c + 1) * tile]).astype(BF16)
    drain(m_send, cols - 1, a2a_send.at[3])


def on_device(rows, cols, *args):
    (
        tokens, outer_weight, inner_weight, value_weight, conv_taps, feature_weight, feature_phase, inner_mats,
        inner_phase, frequency, forward_weight, backward_weight, decay_rate, skip_gain, output_weight,
    ) = args
    length, model = tokens.shape
    width = outer_weight.shape[1]
    units = frequency.shape[0]
    subs = length // LANES
    seq_length = length * rows
    out_rows = length // cols
    operands = (
        tokens, outer_weight.T, inner_weight.T, value_weight.T, conv_taps, feature_weight, feature_phase.reshape(1, units),
        inner_mats, inner_phase, frequency.reshape(1, units), forward_weight.T, backward_weight.T,
        decay_rate.reshape(1, width), skip_gain.reshape(1, width), output_weight,
    ) + tables(rows * subs)
    per = width // (rows // 2)
    held = [
        ((length, model), BF16), ((3 * width, model), BF16), ((3, 3, width), F32), (feature_weight.shape, F32),
        ((1, units), F32), (inner_mats.shape, F32), (inner_phase.shape, F32), ((1, units), F32),
        ((2 * width, units), F32), ((1, width), F32), ((1, width), F32),
    ] + [(x.shape, x.dtype) for x in operands[14:]]
    scratch = [pltpu.VMEM(*x) for x in held] + [
        pltpu.VMEM((length + 16, 3 * width), F32),
        pltpu.VMEM((length, width), F32),
        pltpu.VMEM((length, width), F32),
        pltpu.VMEM((2, width, 2 * subs, LANES), BF16),
        pltpu.VMEM((rows, per, 2 * subs, LANES), BF16),
        pltpu.VMEM((width, 2 * subs, LANES), BF16),
        pltpu.VMEM((rows, per, 2 * subs, LANES), BF16),
        pltpu.VMEM((rows, per, subs, LANES), BF16),
        pltpu.VMEM((width, subs, LANES), BF16),
        pltpu.VMEM((cols, out_rows, width), BF16),
        pltpu.VMEM((cols, out_rows, width), BF16),
        pltpu.SemaphoreType.DMA((24,)),
        pltpu.SemaphoreType.DMA((2,)),
        pltpu.SemaphoreType.DMA((2,)),
        pltpu.SemaphoreType.DMA((4,)),
        pltpu.SemaphoreType.DMA((4,)),
    ]
    return pl.pallas_call(
        functools.partial(kernel, rows, cols, seq_length),
        out_shape=jax.ShapeDtypeStruct((out_rows, model), BF16),
        in_specs=[pl.BlockSpec(memory_space=pl.ANY)] * len(operands),
        out_specs=pl.BlockSpec(memory_space=pltpu.VMEM),
        scratch_shapes=scratch,
        compiler_params=pltpu.CompilerParams(
            collective_id=0, has_side_effects=True, vmem_limit_bytes=56 * 1024 * 1024
        ),
    )(*operands)


def solution(mesh):
    placed = (
        P("row", None),
        P(None, "col"),
        P(None, "col"),
        P(None, "col"),
        P(None, None, "col"),
        P(),
        P(),
        P(),
        P(),
        P(),
        P(None, "col"),
        P(None, "col"),
        P("col"),
        P("col"),
        P(),
    )
    return jax.shard_map(
        functools.partial(on_device, mesh.shape["row"], mesh.shape["col"]),
        mesh=mesh, in_specs=placed, out_specs=P(("row", "col"), None), check_vma=False,
    )
```

time: 67.8 us -> 51.1 us (0.75)
  local copies, waits for them, and re-layouts: 10.4 us -> 1.57 us
  Pallas kernels: 57 us -> 49.4 us
    unnamed x6 -> x1, local copies, waits for them, and re-layouts: 10.4 us -> 1.57 us
    pallas_call x1, Pallas kernels: 57 us -> 49.4 us  [on_device(): pl.pallas_call(functools.partial(kernel, rows, cols, seq_length), out_sha...]
where the time goes in v1:
time: 51.1 us; the launch traced here: 51 us
  Pallas kernels  49.4 us (97%)
  local copies, waits for them, and re-layouts  1.57 us (3%)
    pallas_call x1, Pallas kernels, on_device(): pl.pallas_call(functools.partial(kernel, rows, cols, seq_length), out_sha...  49.4 us
    unnamed x1, local copies, waits for them, and re-layouts  1.57 us

profile of v1, /device:TPU:1, one launch (start us, length us, event | category | flops | bytes accessed | tf_op | source)
XLA Modules:
  0.0 51.0 jit_solution(16607707824002529080)
XLA Ops:
  0.0 49.4 %shard_map.190 = bf16[32,2048]{1,0:T(8,128)(2,1)} custom-call(bf16[512,2048]{1,0:T(8,128)(2,1)} %refs_0_.1, bf16[64,2048]{1,0:T(8,128)(2,1)} %bitcast.9, bf16[64,2048]{1,0:T(8,128)(2,1)} %bitcast.10, bf16[64,2048]{1,0:T(8,128)(2,1)} %bitcast.11, f32[3,3,64]{2,1,0:T(4,128)} %refs_4_.1, f32[33,128]{1,0:T(8,128)} %refs_5_.1, f32[1,128]{1,0:T(1,128)} %bitcast.14, ...), custom_call_target="tpu_custom_call" | custom-call | tf_op jit(solution)/shard_map/pallas_call | solution.py:428
  49.4 1.6 %copy.22 = bf16[32,2048]{1,0:T(8,128)(2,1)} copy(bf16[32,2048]{1,0:T(8,128)(2,1)} %shard_map.190) | data formatting | bytes 262144

commit v2 on v1

--- a/solution.py
+++ b/solution.py
@@ -52,25 +52,20 @@
     return high, (x - high.astype(F32)).astype(BF16)
 
 
-def sine_near(x):
-    x = jnp.maximum(jnp.minimum(x, math.pi - x), -math.pi - x)
+TURN = 2.0 * math.pi
+
+
+def sine_turns(x):
+    x = jnp.maximum(jnp.minimum(x, 0.5 - x), -0.5 - x)
     y = x * x
-    p = y * (2.6083159809786593e-6) - 1.9810690719168633e-4
-    p = p * y + 8.333078585565090e-3
-    p = p * y - 1.6666659712791443e-1
-    return x + x * (y * p)
+    p = y * (2.6083159809786593e-6 * TURN**9) - 1.9810690719168633e-4 * TURN**7
+    p = p * y + 8.333078585565090e-3 * TURN**5
+    p = p * y - 1.6666659712791443e-1 * TURN**3
+    return x * (p * y + TURN)
 
 
 def sine(x):
-    turns = jnp.round(x * (0.5 / math.pi))
-    x = x - turns * 6.28125
-    x = x - turns * 1.93500518798828125e-3
-    x = x - turns * 3.0199159819567530e-7
-    return sine_near(x)
-
-
-def spread(i, size):
-    return size // 2 + ((i + 1) // 2) * (1 - 2 * lax.rem(i, 2))
+    return sine_turns(x - jnp.round(x))
 
 
 def kernel(rows, cols, seq_length, *refs):
@@ -81,7 +76,7 @@
         tok, w_all, taps, first, phase, mats, iphase, freq, both, rate, skip,
         out_w, one, one_back, two, two_back, twist,
         proj, gate_s, sig_s, f_send, f_recv, s_send, s_recv, y_send, y_recv, m_send, m_recv,
-        load_sem, halo_send, halo_recv, a2a_send, a2a_recv,
+        load_sem, halo_send, halo_recv, a2a_send, a2a_recv, hello,
     ) = refs
     me_r, me_c = lax.axis_index("row"), lax.axis_index("col")
     length = tok.shape[0]
@@ -91,13 +86,11 @@
     per = width // zone
     ring = 8 if rows % 8 == 0 else 2
     me_z, me_y = me_r // ring, lax.rem(me_r, ring)
-    after, before = lax.rem(me_r + 1, rows), lax.rem(me_r + rows - 1, rows)
+    after, before = me_r + 1, me_r - 1
     in_zone = me_r < zone
 
     def load(src, dst, index):
-        copy = pltpu.make_async_copy(src, dst, load_sem.at[index])
-        copy.start()
-        return copy
+        return pltpu.make_async_copy(src, dst, load_sem.at[index])
 
     small = [
         load(s, d, i)
@@ -109,44 +102,86 @@
         )
     ]
     weights = [load(w, w_all.at[pl.ds(i * width, width)], 8 + i) for i, w in enumerate((inner_w, value_w, outer_w))]
-    token_load = load(tokens, tok, 11)
+    depth = tok.shape[1]
+    chunks = [(0, depth * 3 // 4), (depth * 3 // 4, depth // 4)]
+    token_loads = [
+        load(tokens.at[:, pl.ds(*c)], tok.at[:, pl.ds(*c)], 11 + i) for i, c in enumerate(chunks)
+    ]
+
+    @pl.when(in_zone)
+    def _():
+        for copy in small:
+            copy.start()
+
+    for copy in weights + token_loads:
+        copy.start()
 
     barrier = pltpu.get_barrier_semaphore()
 
     def greet(row, col):
         pl.semaphore_signal(barrier, inc=1, device_id=(row, col), device_id_type=MESH)
 
-    @pl.when(in_zone)
-    def _():
-        def greet_row(d, carry):
-            greet(lax.rem(me_r + d, rows), me_c)
-            return carry
-
-        lax.fori_loop(1, rows, greet_row, 0)
+    edge = jnp.zeros((8, proj.shape[1]), F32)
+    proj[0:8, :] = edge
+    proj[8 + length : 16 + length, :] = edge
+
+    @pl.when(in_zone)
+    def _():
+        for d in range(1, zone):
+            greet(lax.rem(me_r + d, zone), me_c)
 
     @pl.when(me_r >= zone)
     def _():
         greet(before, me_c)
-        greet(after, me_c)
-
-    def greet_col(i, carry):
-        greet(me_r, lax.rem(me_c + spread(i, cols), cols))
-        return carry
-
-    lax.fori_loop(0, cols - 1, greet_col, 0)
-
-    for copy in small:
-        copy.wait()
-
-    @pl.when(in_zone)
-    def _():
+        pl.when(me_r < rows - 1)(lambda: greet(after, me_c))
+
+    me_x, core = me_c // 2, lax.rem(me_c, 2)
+    chips = cols // 2
+    far = chips // 2
+    steps = [0] + [d for i in range(1, far + 1) for d in ([i] if 2 * i == chips else [i, chips - i])]
+
+    def col_group(distance):
+        if distance == 0:
+            return [2 * me_x + 1 - core]
+        return [2 * lax.rem(me_x + d, chips) + c for d in steps if min(d, chips - d) == distance for c in range(2)]
+
+    def place_in_col(col):
+        x = col // 2
+        return 2 * (x + (x // max(far, 1)) * (chips + far - 1 - 2 * x)) + lax.rem(col, 2)
+
+    my_place = place_in_col(me_c)
+    col_peers = [peer for distance in range(far, -1, -1) for peer in col_group(distance)]
+    for peer in col_peers:
+        pl.when(my_place < place_in_col(peer))(functools.partial(greet, me_r, peer))
+
+    def push(src, dst, index, row):
+        pltpu.make_async_remote_copy(
+            src, dst, a2a_send.at[index], a2a_recv.at[index], device_id=(row, me_c), device_id_type=MESH
+        ).start()
+
+    def drain(ref, count, sem):
+        pltpu.make_async_copy(ref.at[pl.ds(0, count)], ref.at[pl.ds(0, count)], sem).wait()
+
+    def enter():
+        late_before = me_r // (zone + 1)
+        late_after = (me_r + 1) // zone - 2 * ((me_r + 1) // rows)
+        pl.semaphore_wait(barrier, zone - 1 + me_r // zone + late_before + late_after + my_place)
+
+    mine = pl.ds(per * me_r, per)
+
+    @pl.when(in_zone)
+    def _():
+        for copy in small:
+            copy.wait()
         lane = lax.broadcasted_iota(jnp.int32, (length, LANES), 1)
         is_sine = lane > BANDS
         band = 1 + jnp.where(is_sine, lane - (BANDS + 1), lane - 1) * (seq_length // (4 * BANDS))
         shift = jnp.where(is_sine, seq_length, seq_length * 3 // 4)
         rates = jnp.broadcast_to(jnp.concatenate([rate[...], rate[...]], axis=1), (2 * width, 2 * width)).T[:, :1]
         behind = lax.broadcasted_iota(jnp.int32, (2 * width, length), 0) >= width
-        w_first, w_mats, w_both = split(first[...]), split(mats[...]), split(both[...])
+        pace = freq[...] * (1.0 / TURN)
+        w_first, w_both = split(first[...] * pace), split(both[...])
+        w_mats = [split(mats[level] * pace) for level in range(INNER)]
 
         def dot3(x, w, multiply):
             x_high, x_low = split(x)
@@ -156,12 +191,11 @@
             start = (me_r + block * zone) * length
             place = start + lax.broadcasted_iota(jnp.int32, (length, LANES), 0)
             turns = ((place * band + shift) & (seq_length - 1)) - seq_length // 2
-            waves = sine_near(turns.astype(F32) * (2.0 * math.pi / seq_length))
+            waves = sine_turns(turns.astype(F32) * (1.0 / seq_length))
             features = jnp.where(lane == 0, place.astype(F32) / (seq_length - 1), waves)[:, : 2 * BANDS + 1]
-            hidden = sine(freq[...] * (dot3(features, w_first, mm) + phase[...]))
+            hidden = sine(dot3(features, w_first, mm) + pace * phase[...])
             for level in range(INNER):
-                mat = (w_mats[0][level], w_mats[1][level])
-                hidden = sine(freq[...] * (dot3(hidden, mat, mm) + iphase[level : level + 1, :]))
+                hidden = sine(dot3(hidden, w_mats[level], mm) + pace * iphase[level : level + 1, :])
             turned = dot3(hidden, w_both, lambda h, w: mm_t(w, h))
             lag = start + lax.broadcasted_iota(jnp.int32, (2 * width, length), 1)
             turned = turned * jnp.exp(-(lag.astype(F32) / (seq_length - 1)) * rates)
@@ -171,44 +205,9 @@
                 jnp.concatenate([fa + fb, fa - fb], axis=1).reshape(width, 2 * subs, LANES).astype(BF16)
             )
 
-    for copy in weights:
-        copy.wait()
-    token_load.wait()
-    part = mm_t(tok[...], w_all[...]).astype(BF16)
-    proj[pl.ds(8, length), :] = part.astype(F32)
-    turned = part[:, : 2 * width].astype(F32).T
-    s_send[...] = (
-        jnp.concatenate([turned[:width], turned[width:]], axis=1).reshape(width, 2 * subs, LANES).astype(BF16)
-    )
-
-    outside = me_r // zone
-    pl.semaphore_wait(barrier, zone - 1 + outside + before // zone + after // zone + cols - 1)
-
-    def push(src, dst, index, row):
-        pltpu.make_async_remote_copy(
-            src, dst, a2a_send.at[index], a2a_recv.at[index], device_id=(row, me_c), device_id_type=MESH
-        ).start()
-
-    def drain(ref, count, sem):
-        pltpu.make_async_copy(ref.at[pl.ds(0, count)], ref.at[pl.ds(0, count)], sem).wait()
-
-    mine = pl.ds(per * me_r, per)
-    zone_z = zone // ring
-
-    def signal_peer(i, carry):
-        peer = lax.rem(me_z + i, zone_z) * ring + lax.rem(me_y + spread(i // zone_z, ring), ring)
-
-        @pl.when(peer != me_r)
-        def _():
-            push(s_send.at[pl.ds(per * peer, per)], s_recv.at[me_r], 1, peer)
-
-        return carry
-
-    lax.fori_loop(0, zone, signal_peer, 0)
-
-    @pl.when(in_zone)
-    def _():
-        s_recv[me_r] = s_send[mine]
+        for row in range(zone, rows):
+            greet(row, me_c)
+        enter()
 
         def filter_peer(d, carry):
             peer = lax.rem(me_r + d, zone)
@@ -220,16 +219,66 @@
         f_recv[me_r] = f_send[0, mine]
         f_recv[me_r + zone] = f_send[1, mine]
 
+    for copy in weights:
+        copy.wait()
+    part = 0.0
+    for (start, size), copy in zip(chunks, token_loads):
+        copy.wait()
+        own = slice(start, start + size)
+        part = part + mm_t(tok[:, own], w_all[:, own])
+    proj[pl.ds(8, length), :] = part.astype(BF16).astype(F32)
+    turned = proj[pl.ds(8, length), : 2 * width].T
+    s_send[...] = (
+        jnp.concatenate([turned[:width], turned[width:]], axis=1).reshape(width, 2 * subs, LANES).astype(BF16)
+    )
+
+    @pl.when(me_r >= zone)
+    def _():
+        enter()
+
+    zone_z = zone // ring
+    near_y = [lax.rem(me_y + dy, ring) for dy in range(ring)]
+    order = sorted(range(ring), key=lambda d: -min(d, ring - d))
+
+    def signal_peer(peer):
+        push(s_send.at[pl.ds(per * peer, per)], s_recv.at[me_r], 1, peer)
+
+    for dy in order[:-1]:
+        for z in range(zone_z):
+            signal_peer(z * ring + near_y[dy])
+    for z in range(zone_z):
+        pl.when(me_z != z)(functools.partial(signal_peer, z * ring + me_y))
+
+    @pl.when(in_zone)
+    def _():
+        s_recv[me_r] = s_send[mine]
+
+    def answer(peer):
+        pl.semaphore_signal(hello, inc=1, device_id=(me_r, peer), device_id_type=MESH)
+
+    for peer in col_peers:
+        pl.when(my_place > place_in_col(peer))(functools.partial(answer, peer))
+
     late = [
-        load(s, d, 12 + i)
+        load(s, d, 15 + i)
         for i, (s, d) in enumerate(
             [
                 (taps_h, taps), (skip_h, skip), (one_h, one), (two_h, two), (twist_h, twist),
-                (two_back_h, two_back), (one_back_h, one_back), (map_h, out_w),
+                (two_back_h, two_back), (one_back_h, one_back),
             ]
         )
     ]
 
+    tall = 2 * width
+    map_loads = [
+        load(
+            map_h.at[pl.ds(pl.multiple_of(tall * lax.rem(me_x + d, chips), tall), tall)],
+            out_w.at[pl.ds(i * tall, tall)], 15 + len(late) + i,
+        )
+        for i, d in enumerate(steps)
+    ]
+    for copy in late + map_loads:
+        copy.start()
     up = pltpu.make_async_remote_copy(
         proj.at[pl.ds(length, 8)], proj.at[pl.ds(0, 8)], halo_send.at[0], halo_recv.at[0],
         device_id=(after, me_c), device_id_type=MESH,
@@ -238,9 +287,9 @@
         proj.at[pl.ds(8, 8)], proj.at[pl.ds(8 + length, 8)], halo_send.at[1], halo_recv.at[1],
         device_id=(before, me_c), device_id_type=MESH,
     )
-    up.start()
-    down.start()
-    for copy in late[:7]:
+    pl.when(me_r < rows - 1)(up.start)
+    pl.when(me_r > 0)(down.start)
+    for copy in late:
         copy.wait()
 
     half = rows * subs
@@ -319,22 +368,29 @@
         for c in range(per):
             y_send[:, c] = response[:, c * LANES : (c + 1) * LANES].reshape(rows, subs, LANES).astype(BF16)
 
-        ring_z = rows // ring
-
-        def response_peer(i, carry):
-            peer = lax.rem(me_z + spread(lax.rem(i, ring_z), ring_z), ring_z) * ring + lax.rem(
-                me_y + spread(i // ring_z, ring), ring
-            )
+        def response_peer(peer):
             push(y_send.at[peer], y_recv.at[mine], 2, peer)
-            return carry
-
-        lax.fori_loop(0, rows - 1, response_peer, 0)
+
+        for dy in order:
+            for z in range(zone_z, rows // ring):
+                response_peer(z * ring + near_y[dy])
+        for dy in order[:-1]:
+            for z in range(zone_z):
+                response_peer(z * ring + near_y[dy])
+        for z in range(zone_z):
+            pl.when(me_z != z)(functools.partial(response_peer, z * ring + me_y))
         y_recv[mine] = y_send[me_r]
 
-    up.wait()
-    down.wait()
-    proj[7:8, :] = jnp.where(me_r == 0, 0.0, proj[7:8, :])
-    proj[8 + length : 9 + length, :] = jnp.where(me_r == rows - 1, 0.0, proj[8 + length : 9 + length, :])
+    @pl.when(me_r < rows - 1)
+    def _():
+        up.wait_send()
+        down.wait_recv()
+
+    @pl.when(me_r > 0)
+    def _():
+        down.wait_send()
+        up.wait_recv()
+
     tap = [
         jnp.concatenate([taps[a, 1:2, :], taps[a, 2:3, :], taps[a, 0:1, :]], axis=1) for a in range(3)
     ]
@@ -342,7 +398,8 @@
     signal = (conv[:, :width] * conv[:, width : 2 * width]).astype(BF16).astype(F32)
     gate_s[...] = conv[:, 2 * width :].astype(BF16).astype(F32)
     sig_s[...] = skip[...] * signal
-    late[7].wait()
+    for copy in map_loads:
+        copy.wait()
 
     @pl.when(in_zone)
     def _():
@@ -354,17 +411,17 @@
 
     replied = y_recv[...].astype(F32).reshape(width, length).T
     mixed = (gate_s[...] * (replied + sig_s[...])).astype(BF16)
-    m_send[...] = mixed.reshape(cols, length // cols, width)
-
-    def col_peer(i, carry):
-        peer = lax.rem(me_c + spread(i, cols), cols)
-        pltpu.make_async_remote_copy(
-            m_send.at[peer], m_recv.at[me_c], a2a_send.at[3], a2a_recv.at[3],
-            device_id=(me_r, peer), device_id_type=MESH,
-        ).start()
-        return carry
-
-    lax.fori_loop(0, cols - 1, col_peer, 0)
+    thin = length // cols // 2
+    mixed = mixed.reshape(cols, 2, thin, width)
+    m_send[...] = jnp.concatenate([mixed[:, 0], mixed[:, 1]], axis=2)
+
+    pl.when(my_place < cols - 1)(lambda: pl.semaphore_wait(hello, cols - 1 - my_place))
+    for distance in range(far, -1, -1):
+        for peer in col_group(distance):
+            pltpu.make_async_remote_copy(
+                m_send.at[peer], m_recv.at[me_c], a2a_send.at[3], a2a_recv.at[3 + distance],
+                device_id=(me_r, peer), device_id_type=MESH,
+            ).start()
     m_recv[me_c] = m_send[me_c]
 
     @pl.when(in_zone)
@@ -377,11 +434,23 @@
     def _():
         drain(s_send, width, a2a_send.at[1])
 
-    drain(m_recv, cols - 1, a2a_recv.at[3])
-    whole = jnp.concatenate([m_recv[j] for j in range(cols)], axis=1)
-    tile = min(512, out_ref.shape[1])
-    for c in range(out_ref.shape[1] // tile):
-        out_ref[:, c * tile : (c + 1) * tile] = mm(whole, out_w[:, c * tile : (c + 1) * tile]).astype(BF16)
+    total = None
+    done = 0
+    for group in [list(range(min(2, far + 1)))] + [[d] for d in range(2, far + 1)]:
+        count = 0
+        for distance in group:
+            drain(m_recv, len(col_group(distance)), a2a_recv.at[3 + distance])
+            count += sum(min(d, chips - d) == distance for d in steps)
+        chosen = [lax.rem(me_x + d, chips) for d in steps[done : done + count]]
+        slabs = [m_recv[2 * x + c] for x in chosen for c in range(2)]
+        gathered = jnp.concatenate(
+            [jnp.concatenate([slab[:, own] for slab in slabs], axis=1) for own in (slice(0, width), slice(width, tall))],
+            axis=0,
+        )
+        term = mm(gathered, out_w[done * tall : (done + count) * tall, :])
+        total = term if total is None else total + term
+        done += count
+    out_ref[...] = total.astype(BF16)
     drain(m_send, cols - 1, a2a_send.at[3])
 
 
@@ -417,17 +486,18 @@
         pltpu.VMEM((rows, per, 2 * subs, LANES), BF16),
         pltpu.VMEM((rows, per, subs, LANES), BF16),
         pltpu.VMEM((width, subs, LANES), BF16),
-        pltpu.VMEM((cols, out_rows, width), BF16),
-        pltpu.VMEM((cols, out_rows, width), BF16),
-        pltpu.SemaphoreType.DMA((24,)),
+        pltpu.VMEM((cols, out_rows // 2, 2 * width), BF16),
+        pltpu.VMEM((cols, out_rows // 2, 2 * width), BF16),
+        pltpu.SemaphoreType.DMA((32,)),
         pltpu.SemaphoreType.DMA((2,)),
         pltpu.SemaphoreType.DMA((2,)),
         pltpu.SemaphoreType.DMA((4,)),
-        pltpu.SemaphoreType.DMA((4,)),
+        pltpu.SemaphoreType.DMA((4 + cols // 4,)),
+        pltpu.SemaphoreType.REGULAR,
     ]
     return pl.pallas_call(
         functools.partial(kernel, rows, cols, seq_length),
-        out_shape=jax.ShapeDtypeStruct((out_rows, model), BF16),
+        out_shape=pltpu.VMEM((out_rows, model), BF16),
         in_specs=[pl.BlockSpec(memory_space=pl.ANY)] * len(operands),
         out_specs=pl.BlockSpec(memory_space=pltpu.VMEM),
         scratch_shapes=scratch,

time: 51.1 us -> 45.9 us (0.90)
  Pallas kernels: 49.4 us -> 45.1 us
  local copies, waits for them, and re-layouts: 1.57 us -> 0.66 us
    pallas_call x1, Pallas kernels: 49.4 us -> 45.1 us  [on_device(): pl.pallas_call(functools.partial(kernel, rows, cols, seq_length), out_sha...]
    unnamed x1, local copies, waits for them, and re-layouts: 1.57 us -> 0.66 us
where the time goes in v2:
time: 45.9 us; the launch traced here: 45.8 us
  Pallas kernels  45.1 us (98%)
  local copies, waits for them, and re-layouts  0.66 us (1%)
    pallas_call x1, Pallas kernels, on_device(): pl.pallas_call(functools.partial(kernel, rows, cols, seq_length), out_sha...  45.1 us

profile of v2, /device:TPU:1, one launch (start us, length us, event | category | flops | bytes accessed | tf_op | source)
XLA Modules:
  0.0 45.8 jit_solution(13785951514809391347)
XLA Ops:
  0.0 45.1 %shard_map.190 = bf16[32,2048]{1,0:T(8,128)(2,1)S(1)} custom-call(bf16[512,2048]{1,0:T(8,128)(2,1)} %refs_0_.1, bf16[64,2048]{1,0:T(8,128)(2,1)} %bitcast.9, bf16[64,2048]{1,0:T(8,128)(2,1)} %bitcast.10, bf16[64,2048]{1,0:T(8,128)(2,1)} %bitcast.11, f32[3,3,64]{2,1,0:T(4,128)} %refs_4_.1, f32[33,128]{1,0:T(8,128)} %refs_5_.1, f32[1,128]{1,0:T(1,128)} %bitcast.14, ...), custom_call_target="tpu_custom_call" | custom-call | tf_op jit(solution)/shard_map/pallas_call | solution.py:498
  45.1 0.7 %copy.22 = bf16[32,2048]{1,0:T(8,128)(2,1)} copy(bf16[32,2048]{1,0:T(8,128)(2,1)S(1)} %shard_map.190) | data formatting | bytes 262144

commit v3 on v2

--- a/solution.py
+++ b/solution.py
@@ -88,6 +88,9 @@
     me_z, me_y = me_r // ring, lax.rem(me_r, ring)
     after, before = me_r + 1, me_r - 1
     in_zone = me_r < zone
+    zone_z = zone // ring
+    near_y = [lax.rem(me_y + dy, ring) for dy in range(ring)]
+    order = sorted(range(ring), key=lambda d: -min(d, ring - d))
 
     def load(src, dst, index):
         return pltpu.make_async_copy(src, dst, load_sem.at[index])
@@ -102,11 +105,8 @@
         )
     ]
     weights = [load(w, w_all.at[pl.ds(i * width, width)], 8 + i) for i, w in enumerate((inner_w, value_w, outer_w))]
-    depth = tok.shape[1]
-    chunks = [(0, depth * 3 // 4), (depth * 3 // 4, depth // 4)]
-    token_loads = [
-        load(tokens.at[:, pl.ds(*c)], tok.at[:, pl.ds(*c)], 11 + i) for i, c in enumerate(chunks)
-    ]
+    high = length // 8
+    token_loads = [load(tokens.at[pl.ds(i * high, high)], tok.at[pl.ds(i * high, high)], 11 + i) for i in range(8)]
 
     @pl.when(in_zone)
     def _():
@@ -129,6 +129,12 @@
     def _():
         for d in range(1, zone):
             greet(lax.rem(me_r + d, zone), me_c)
+
+    def greet_late():
+        for row in range(zone, rows):
+            greet(row, me_c)
+
+    pl.when(me_z == zone_z - 1)(greet_late)
 
     @pl.when(me_r >= zone)
     def _():
@@ -205,28 +211,25 @@
                 jnp.concatenate([fa + fb, fa - fb], axis=1).reshape(width, 2 * subs, LANES).astype(BF16)
             )
 
-        for row in range(zone, rows):
-            greet(row, me_c)
+        pl.when(me_z < zone_z - 1)(greet_late)
         enter()
 
-        def filter_peer(d, carry):
-            peer = lax.rem(me_r + d, zone)
+        def filter_peer(peer):
             push(f_send.at[0, pl.ds(per * peer, per)], f_recv.at[me_r], 0, peer)
             push(f_send.at[1, pl.ds(per * peer, per)], f_recv.at[me_r + zone], 0, peer)
-            return carry
-
-        lax.fori_loop(1, zone, filter_peer, 0)
+
+        for z in reversed(range(zone_z)):
+            for dy in order[:-1]:
+                filter_peer(z * ring + near_y[dy])
+            pl.when(me_z != z)(functools.partial(filter_peer, z * ring + me_y))
         f_recv[me_r] = f_send[0, mine]
         f_recv[me_r + zone] = f_send[1, mine]
 
     for copy in weights:
         copy.wait()
-    part = 0.0
-    for (start, size), copy in zip(chunks, token_loads):
+    for copy in token_loads:
         copy.wait()
-        own = slice(start, start + size)
-        part = part + mm_t(tok[:, own], w_all[:, own])
-    proj[pl.ds(8, length), :] = part.astype(BF16).astype(F32)
+    proj[pl.ds(8, length), :] = mm_t(tok[...], w_all[...]).astype(BF16).astype(F32)
     turned = proj[pl.ds(8, length), : 2 * width].T
     s_send[...] = (
         jnp.concatenate([turned[:width], turned[width:]], axis=1).reshape(width, 2 * subs, LANES).astype(BF16)
@@ -236,17 +239,13 @@
     def _():
         enter()
 
-    zone_z = zone // ring
-    near_y = [lax.rem(me_y + dy, ring) for dy in range(ring)]
-    order = sorted(range(ring), key=lambda d: -min(d, ring - d))
 
     def signal_peer(peer):
         push(s_send.at[pl.ds(per * peer, per)], s_recv.at[me_r], 1, peer)
 
-    for dy in order[:-1]:
-        for z in range(zone_z):
+    for z in reversed(range(zone_z)):
+        for dy in order[:-1]:
             signal_peer(z * ring + near_y[dy])
-    for z in range(zone_z):
         pl.when(me_z != z)(functools.partial(signal_peer, z * ring + me_y))
 
     @pl.when(in_zone)
@@ -260,7 +259,7 @@
         pl.when(my_place > place_in_col(peer))(functools.partial(answer, peer))
 
     late = [
-        load(s, d, 15 + i)
+        load(s, d, 19 + i)
         for i, (s, d) in enumerate(
             [
                 (taps_h, taps), (skip_h, skip), (one_h, one), (two_h, two), (twist_h, twist),
@@ -273,7 +272,7 @@
     map_loads = [
         load(
             map_h.at[pl.ds(pl.multiple_of(tall * lax.rem(me_x + d, chips), tall), tall)],
-            out_w.at[pl.ds(i * tall, tall)], 15 + len(late) + i,
+            out_w.at[pl.ds(i * tall, tall)], 19 + len(late) + i,
         )
         for i, d in enumerate(steps)
     ]
@@ -371,13 +370,9 @@
         def response_peer(peer):
             push(y_send.at[peer], y_recv.at[mine], 2, peer)
 
-        for dy in order:
-            for z in range(zone_z, rows // ring):
+        for z in range(rows // ring):
+            for dy in order[:-1]:
                 response_peer(z * ring + near_y[dy])
-        for dy in order[:-1]:
-            for z in range(zone_z):
-                response_peer(z * ring + near_y[dy])
-        for z in range(zone_z):
             pl.when(me_z != z)(functools.partial(response_peer, z * ring + me_y))
         y_recv[mine] = y_send[me_r]
 
@@ -488,7 +483,7 @@
         pltpu.VMEM((width, subs, LANES), BF16),
         pltpu.VMEM((cols, out_rows // 2, 2 * width), BF16),
         pltpu.VMEM((cols, out_rows // 2, 2 * width), BF16),
-        pltpu.SemaphoreType.DMA((32,)),
+        pltpu.SemaphoreType.DMA((40,)),
         pltpu.SemaphoreType.DMA((2,)),
         pltpu.SemaphoreType.DMA((2,)),
         pltpu.SemaphoreType.DMA((4,)),

time: 45.9 us -> 44.6 us (0.972)
  Pallas kernels: 45.1 us -> 43.7 us
    pallas_call x1, Pallas kernels: 45.1 us -> 43.7 us  [on_device(): pl.pallas_call(functools.partial(kernel, rows, cols, seq_length), out_sha...]
where the time goes in v3:
time: 44.6 us; the launch traced here: 44.4 us
  Pallas kernels  43.7 us (98%)
  local copies, waits for them, and re-layouts  0.66 us (1%)
    pallas_call x1, Pallas kernels, on_device(): pl.pallas_call(functools.partial(kernel, rows, cols, seq_length), out_sha...  43.7 us

profile of v3, /device:TPU:1, one launch (start us, length us, event | category | flops | bytes accessed | tf_op | source)
XLA Modules:
  0.0 44.4 jit_solution(10355027439661206128)
XLA Ops:
  0.0 43.7 %shard_map.190 = bf16[32,2048]{1,0:T(8,128)(2,1)S(1)} custom-call(bf16[512,2048]{1,0:T(8,128)(2,1)} %refs_0_.1, bf16[64,2048]{1,0:T(8,128)(2,1)} %bitcast.9, bf16[64,2048]{1,0:T(8,128)(2,1)} %bitcast.10, bf16[64,2048]{1,0:T(8,128)(2,1)} %bitcast.11, f32[3,3,64]{2,1,0:T(4,128)} %refs_4_.1, f32[33,128]{1,0:T(8,128)} %refs_5_.1, f32[1,128]{1,0:T(1,128)} %bitcast.14, ...), custom_call_target="tpu_custom_call" | custom-call | tf_op jit(solution)/shard_map/pallas_call | solution.py:493
  43.7 0.7 %copy.22 = bf16[32,2048]{1,0:T(8,128)(2,1)} copy(bf16[32,2048]{1,0:T(8,128)(2,1)S(1)} %shard_map.190) | data formatting | bytes 262144

commit v4 on v3

--- a/solution.py
+++ b/solution.py
@@ -326,17 +326,23 @@
         row = lax.broadcasted_iota(jnp.int32, (half, LANES), 0)
         channel = lax.broadcasted_iota(jnp.int32, (1, width), 1)
 
+        own_taps = {
+            (which, c): [
+                jnp.sum(jnp.where(channel == per * me_r + c, taps[a, which : which + 1, :], 0.0), axis=1, keepdims=True)
+                for a in range(3)
+            ]
+            for which in (1, 2)
+            for c in range(per)
+        }
+
         def short_conv(x, which, c):
+            tap = own_taps[which, c]
             left = pltpu.roll(x, 1, 1)
             left = jnp.where(lane == 0, pltpu.roll(left, 1, 0), left)
             left = jnp.where((lane == 0) & (row == 0), 0.0, left)
             right = pltpu.roll(x, LANES - 1, 1)
             right = jnp.where(lane == LANES - 1, pltpu.roll(right, half - 1, 0), right)
             right = jnp.where((lane == LANES - 1) & (row == half - 1), 0.0, right)
-            tap = [
-                jnp.sum(jnp.where(channel == per * me_r + c, taps[a, which : which + 1, :], 0.0), axis=1, keepdims=True)
-                for a in range(3)
-            ]
             return left * tap[0] + x * tap[1] + right * tap[2]
 
         drain(s_recv, rows - 1, a2a_recv.at[1])

time: 44.6 us -> 44.5 us (level)
  no operation moved by 1% of the time
where the time goes in v4:
time: 44.5 us; the launch traced here: 44.4 us
  Pallas kernels  43.7 us (98%)
  local copies, waits for them, and re-layouts  0.66 us (1%)
    pallas_call x1, Pallas kernels, on_device(): pl.pallas_call(functools.partial(kernel, rows, cols, seq_length), out_sha...  43.7 us

profile of v4, /device:TPU:1, one launch (start us, length us, event | category | flops | bytes accessed | tf_op | source)
XLA Modules:
  0.0 44.4 jit_solution(11952549007537307451)
XLA Ops:
  0.0 43.7 %shard_map.190 = bf16[32,2048]{1,0:T(8,128)(2,1)S(1)} custom-call(bf16[512,2048]{1,0:T(8,128)(2,1)} %refs_0_.1, bf16[64,2048]{1,0:T(8,128)(2,1)} %bitcast.9, bf16[64,2048]{1,0:T(8,128)(2,1)} %bitcast.10, bf16[64,2048]{1,0:T(8,128)(2,1)} %bitcast.11, f32[3,3,64]{2,1,0:T(4,128)} %refs_4_.1, f32[33,128]{1,0:T(8,128)} %refs_5_.1, f32[1,128]{1,0:T(1,128)} %bitcast.14, ...), custom_call_target="tpu_custom_call" | custom-call | tf_op jit(solution)/shard_map/pallas_call | solution.py:499
  43.7 0.7 %copy.22 = bf16[32,2048]{1,0:T(8,128)(2,1)} copy(bf16[32,2048]{1,0:T(8,128)(2,1)S(1)} %shard_map.190) | data formatting | bytes 262144
